TPU v7x, 32 devices: a whole 2x2x4 slice. The times are simulated.
32 devices in a mesh: sp: 4 (over y, x), tp: 8 (over z, core).
Axes of the slice: x: 2, y: 2, z: 4, core: 2. Of those that a mesh axis runs over, the one named last changes fastest.
Arguments:
- gate_b: bfloat16 [2048, 1024], P('sp', 'tp'), may hold values from -6 to 6
- gate_c: bfloat16 [2048, 1024], P('sp', 'tp'), may hold values from -6 to 6
- values_in: bfloat16 [2048, 1024], P('sp', 'tp'), may hold values from -6 to 6
- conv_w: bfloat16 [3, 1024], P(None, 'tp'), may hold values from -3.5 to 3.5
- documents: int32 [2048], P('sp'), may hold values from 0 to 2, never falling along the last dimension, each value on 1 to 1024 neighbouring positions
- w_out: bfloat16 [1024, 2048], replicated, may hold values from -0.1875 to 0.1875
- resid: bfloat16 [2048, 2048], P(('sp', 'tp')), may hold values from -6 to 6
- norm_gain: bfloat16 [2048], replicated, may hold values from 0.099609375 to 1.8984375
- route_ids: int32 [2048, 2], P(('sp', 'tp')), may hold values from 0 to 3, all different within a row; in each aligned block of 64 rows (0 to 63, 64 to 127, ...) at most 64 rows name the same one
- route_weight: float32 [2048, 2], P(('sp', 'tp')), may hold values from 0.2 to 1
- w_gate: bfloat16 [4, 2048, 7168], P('sp', None, 'tp'), may hold values from -0.125 to 0.125
- w_up: bfloat16 [4, 2048, 7168], P('sp', None, 'tp'), may hold values from -0.125 to 0.125
- w_down: bfloat16 [4, 7168, 2048], P('sp', 'tp'), may hold values from -0.0625 to 0.0625
Outputs:
- layer_out: bfloat16 [2048, 2048], P(('sp', 'tp'))
Inputs may be any that keep to these rules, and one draw needn't show every extreme that they name: `route_ids`: each token names two different experts; in the rows of one device no expert is named by more than 64 rows, a bound that some block reaches. `documents`: document numbers never fall along the positions; a document has at most 2048 // 2 positions.
All inputs are finite; a program needn't handle non-finite values.
Results may differ from a plain program's by a relative error of at most 0.018.
Values may be sent and summed in bfloat16 or wider, within the bound.
A program may use at most 128 MiB of HBM per device.

v0:
```python
import jax
import jax.numpy as jnp
from jax import lax
from jax.sharding import PartitionSpec as P


def passed_along(block, axis, distance):
    devices = range(lax.axis_size(axis))
    route = [(i - distance, i) for i in devices if i - distance in devices]
    return lax.ppermute(block, axis, route)


def local(
    gate_b,
    gate_c,
    values_in,
    conv_w,
    documents,
    w_out,
    resid,
    norm_gain,
    route_ids,
    route_weight,
    w_gate,
    w_up,
    w_down,
):
    seq_rows = gate_b.shape[0]
    local_rows = resid.shape[0]
    model_width = resid.shape[1]
    last_rows = jnp.stack([gate_c[seq_rows - 2 :], values_in[seq_rows - 2 :]])
    before, before_docs = passed_along((last_rows, documents[seq_rows - 2 :]), "sp", 1)
    products = jnp.concatenate(
        [
            before[0].astype(jnp.float32) * before[1].astype(jnp.float32),
            gate_c.astype(jnp.float32) * values_in.astype(jnp.float32),
        ],
        axis=0,
    )
    docs_all = jnp.concatenate([before_docs, documents], axis=0)
    kernel_taps = conv_w.astype(jnp.float32)
    near_mask = (docs_all[1:-1] == documents).astype(jnp.float32)[:, None]
    far_mask = (docs_all[:-2] == documents).astype(jnp.float32)[:, None]
    convolved = (
        kernel_taps[2] * products[2:]
        + kernel_taps[1] * products[1:-1] * near_mask
        + kernel_taps[0] * products[:-2] * far_mask
    )
    mixed_rows = (gate_b.astype(jnp.float32) * convolved).astype(jnp.bfloat16)
    token_rows = lax.all_to_all(mixed_rows, "tp", split_axis=0, concat_axis=1, tiled=True)
    projected = jnp.dot(token_rows, w_out, preferred_element_type=jnp.float32)
    hidden_state = (resid.astype(jnp.float32) + projected).astype(jnp.bfloat16)
    state_wide = hidden_state.astype(jnp.float32)
    normed = (
        state_wide
        * lax.rsqrt(jnp.mean(state_wide * state_wide, axis=-1, keepdims=True) + 1e-06)
        * norm_gain.astype(jnp.float32)
    ).astype(jnp.bfloat16)
    experts = lax.axis_size("sp") * w_gate.shape[0]
    capacity = 4 * local_rows // experts
    flat_ids = route_ids.reshape(-1)
    one_hot = (flat_ids[:, None] == jnp.arange(experts, dtype=jnp.int32)[None, :]).astype(jnp.int32)
    rank_in = jnp.sum((jnp.cumsum(one_hot, axis=0) - one_hot) * one_hot, axis=1)
    slot_index = flat_ids * capacity + rank_in
    placement = (
        slot_index[:, None] == jnp.arange(experts * capacity, dtype=jnp.int32)[None, :]
    ).astype(jnp.bfloat16)
    repeated = jnp.repeat(normed, 2, axis=0)
    dispatch = jnp.einsum(
        "js,jd->sd", placement, repeated, preferred_element_type=jnp.float32
    ).astype(jnp.bfloat16)
    dispatch = dispatch.reshape(experts, capacity, model_width)
    gathered_piece = lax.all_gather(
        lax.all_to_all(dispatch, "sp", split_axis=0, concat_axis=0, tiled=True),
        "tp",
        axis=0,
        tiled=True,
    )
    flat_rows = gathered_piece.reshape(-1, model_width)
    gate_part = jnp.dot(flat_rows, w_gate[0], preferred_element_type=jnp.float32)
    up_part = jnp.dot(flat_rows, w_up[0], preferred_element_type=jnp.float32)
    activated = (jax.nn.silu(gate_part) * up_part).astype(jnp.bfloat16)
    partial_value = jnp.dot(activated, w_down[0], preferred_element_type=jnp.float32)
    partial_value = partial_value.reshape(
        gathered_piece.shape[0], gathered_piece.shape[1], model_width
    )
    summed = lax.psum_scatter(
        partial_value.astype(jnp.bfloat16), "tp", scatter_dimension=0, tiled=True
    )
    returned = lax.all_to_all(summed, "sp", split_axis=0, concat_axis=0, tiled=True)
    picked = jnp.take(
        returned.reshape(experts * capacity, model_width), slot_index, axis=0
    ).reshape(local_rows, 2, model_width)
    combined = jnp.sum(route_weight[:, :, None] * picked.astype(jnp.float32), axis=1)
    return (hidden_state.astype(jnp.float32) + combined).astype(jnp.bfloat16)


def solution(mesh):
    return jax.shard_map(
        local,
        mesh=mesh,
        in_specs=(
            P("sp", "tp"),
            P("sp", "tp"),
            P("sp", "tp"),
            P(None, "tp"),
            P("sp"),
            P(),
            P(("sp", "tp"), None),
            P(),
            P(("sp", "tp"), None),
            P(("sp", "tp"), None),
            P("sp", None, "tp"),
            P("sp", None, "tp"),
            P("sp", "tp", None),
        ),
        out_specs=P(("sp", "tp"), None),
        check_vma=False,
    )
```

profile of v0, /device:TPU:10, one launch (start us, length us, event | category | flops | bytes accessed | tf_op | source)
XLA Modules:
  0.0 285.8 jit_solution(4626521209556720587)
XLA Ops:
  6.5 0.7 slice_bitcast_fusion.1
  7.2 3.4 %collective-permute-start = (bf16[2,2,128]{2,1,0:T(2,128)(2,1)S(1)}, bf16[2,2,128]{2,1,0:T(2,128)(2,1)S(1)}, u32[]{:S(2)}, u32[]{:S(2)}) collective-permute-start(bf16[2,2,128]{2,1,0:T(2,128)(2,1)S(1)} %pad_maximum_fusion.1), channel_id=1, source_target_pairs={{0,8},{8,16},{16,24},{1,9},{9,17},{17,25},{2,10},{10,18},{18,26},{... | collective-permute-start | bytes 3080 | tf_op jit(solution)/shard_map/ppermute | solution.py:10
  10.7 0.8 slice.43
  11.4 3.4 %collective-permute-start.1 = (s32[2]{0:T(128)S(1)}, s32[2]{0:T(128)S(1)}, u32[]{:S(2)}, u32[]{:S(2)}) collective-permute-start(s32[2]{0:T(128)S(1)} %slice.43), channel_id=1, source_target_pairs={{0,8},{8,16},{16,24},{1,9},{9,17},{17,25},{2,10},{10,18},{18,26},{... | collective-permute-start | bytes 32 | tf_op jit(solution)/shard_map/ppermute | solution.py:10
  14.8 1.0 convert_multiply_fusion
  15.8 0.7 convert_element_type.66
  16.5 0.8 copy.27
  17.5 0.2 reduce_window_sum.11
  17.7 0.8 pad_add_fusion
  18.4 0.8 fusion.19
  19.2 1.8 fusion.12
  21.0 5.3 %all-to-all-start = ((bf16[8,64,128]{2,1,0:T(8,128)(2,1)}), bf16[8,64,128]{2,1,0:T(8,128)(2,1)S(1)}, u32[]{:S(2)}, u32[]{:S(2)}) async-start(bf16[8,64,128]{2,1,0:T(8,128)(2,1)} %bitcast.6), calls=%async_computation | async-start | bytes 262144 | tf_op jit(solution)/shard_map/all_to_all | solution.py:50
  26.3 0.2 select_reduce_fusion
  26.5 0.7 convert_element_type.77
  27.2 4.8 %all-to-all-done = bf16[8,64,128]{2,1,0:T(8,128)(2,1)S(1)} async-done(((bf16[8,64,128]{2,1,0:T(8,128)(2,1)}), bf16[8,64,128]{2,1,0:T(8,128)(2,1)S(1)}, u32[]{:S(2)}, u32[]{:S(2)}) %all-to-all-start) | async-done | bytes 131104 | tf_op jit(solution)/shard_map/all_to_all | solution.py:50
  31.9 3.2 %multiply_reduce_fusion.1 = (f32[64]{0:T(128)S(1)}, f32[64,2048]{1,0:T(8,128)S(1)}) fusion(bf16[1024,2048]{1,0:T(8,128)(2,1)} %param.18, bf16[64,2048]{1,0:T(8,128)(2,1)} %param.19, bf16[8,64,128]{2,1,0:T(8,128)(2,1)S(1)} %all-to-all-done), kind=kOutput, calls=%fused_computation.15 | convolution fusion | flops 269221824 | bytes 5112064 | tf_op jit(solution)/shard_map/dot_general | solution.py:51
  35.2 0.3 broadcast_in_dim.10
  35.6 0.2 reshape.84
  35.8 0.5 convolution_convert_fusion.1
  36.3 16.8 %all_to_all.29 = bf16[4,64,2048]{2,1,0:T(8,128)(2,1)} all-to-all(bf16[4,64,2048]{2,1,0:T(8,128)(2,1)S(1)} %bitcast.49), channel_id=1, replica_groups=mesh['sp'=4,'tp'=8] {'sp'}, dimensions={0} | all-to-all | bytes 2097152 | tf_op jit(solution)/shard_map/all_to_all | solution.py:74
  53.2 78.4 %all-gather.2.cloned.1.call-done = bf16[32,64,2048]{2,1,0:T(8,128)(2,1)} async-done(((bf16[4,64,2048]{2,1,0:T(8,128)(2,1)}), bf16[32,64,2048]{2,1,0:T(8,128)(2,1)}) %all-gather.2.cloned.1.call-update) | async-done | bytes 8388624 | tf_op jit(solution)/shard_map/all_gather | solution.py:73
  131.6 14.3 %fusion.2 = f32[2048,896]{1,0:T(8,128)} fusion(bf16[2048,2048]{1,0:T(8,128)(2,1)} %bitcast.50, bf16[1,2048,896]{2,1,0:T(8,128)(2,1)} %param.23), kind=kOutput, calls=%fused_computation.5 | convolution fusion | flops 7516192768 | bytes 19398656 | tf_op jit(solution)/shard_map/dot_general | solution.py:80
  145.9 11.3 %multiply_convert_fusion = bf16[2048,896]{1,0:T(8,128)(2,1)S(1)} fusion(f32[2048,896]{1,0:T(8,128)} %fusion.2, bf16[2048,2048]{1,0:T(8,128)(2,1)S(1)} %bitcast.51, bf16[1,2048,896]{2,1,0:T(8,128)(2,1)S(1)} %copy-done.3), kind=kOutput, calls=%fused_computation.1 | convolution fusion | flops 7527202816 | bytes 23068672 | tf_op jit(solution)/shard_map/dot_general | solution.py:81
  157.2 11.0 %convolution_convert_fusion = bf16[32,64,2048]{2,1,0:T(8,128)(2,1)} fusion(bf16[32,64,896]{2,1,0:T(8,128)(2,1)S(1)} %bitcast.52, bf16[1,896,2048]{2,1,0:T(8,128)(2,1)S(1)} %copy-done.4), kind=kOutput, calls=%fused_computation.2 | convolution fusion | flops 7520387072 | bytes 15728640 | tf_op jit(solution)/shard_map/dot_general | solution.py:83
  168.2 87.8 %reduce-scatter.2.cloned.1.call-done = bf16[4,64,2048]{2,1,0:T(8,128)(2,1)} async-done(((bf16[32,64,2048]{2,1,0:T(8,128)(2,1)}), bf16[4,64,2048]{2,1,0:T(8,128)(2,1)}) %reduce-scatter.2.cloned.1.call-update) | async-done | bytes 1048592 | tf_op jit(solution)/shard_map/reduce_scatter | solution.py:87
  256.0 4.2 %all-to-all-start.2 = ((bf16[4,64,2048]{2,1,0:T(8,128)(2,1)}), bf16[4,64,2048]{2,1,0:T(8,128)(2,1)S(1)}, u32[]{:S(2)}, u32[]{:S(2)}) async-start(bf16[4,64,2048]{2,1,0:T(8,128)(2,1)} %reduce-scatter.2.cloned.1.call-done), calls=%async_computation.3 | async-start | bytes 2097152 | tf_op jit(solution)/shard_map/all_to_all | solution.py:90
  260.5 0.1 mul.151
  261.0 13.5 %all-to-all-done.2 = bf16[4,64,2048]{2,1,0:T(8,128)(2,1)S(1)} async-done(((bf16[4,64,2048]{2,1,0:T(8,128)(2,1)}), bf16[4,64,2048]{2,1,0:T(8,128)(2,1)S(1)}, u32[]{:S(2)}, u32[]{:S(2)}) %all-to-all-start.2) | async-done | bytes 1048608 | tf_op jit(solution)/shard_map/all_to_all | solution.py:90
  274.4 0.9 gather_fusion
  275.4 0.3 gather.7
  275.7 2.5 multiply_reduce_fusion
  278.2 0.8 add_convert_fusion
  (33 shorter events, 1.0 us)
Async XLA Ops:
  7.2 11.9 %collective-permute-start = (bf16[2,2,128]{2,1,0:T(2,128)(2,1)S(1)}, bf16[2,2,128]{2,1,0:T(2,128)(2,1)S(1)}, u32[]{:S(2)}, u32[]{:S(2)}) collective-permute-start(bf16[2,2,128]{2,1,0:T(2,128)(2,1)S(1)} %pad_maximum_fusion.1), channel_id=1, source_target_pairs={{0,8},{8,16},{16,24},{1,9},{9,17},{17,25},{2,10},{10,18},{18,26},{... | collective-permute-start | bytes 3080 | tf_op jit(solution)/shard_map/ppermute | solution.py:10
  11.4 6.3 %collective-permute-start.1 = (s32[2]{0:T(128)S(1)}, s32[2]{0:T(128)S(1)}, u32[]{:S(2)}, u32[]{:S(2)}) collective-permute-start(s32[2]{0:T(128)S(1)} %slice.43), channel_id=1, source_target_pairs={{0,8},{8,16},{16,24},{1,9},{9,17},{17,25},{2,10},{10,18},{18,26},{... | collective-permute-start | bytes 32 | tf_op jit(solution)/shard_map/ppermute | solution.py:10
  21.0 11.0 %all-to-all-start = ((bf16[8,64,128]{2,1,0:T(8,128)(2,1)}), bf16[8,64,128]{2,1,0:T(8,128)(2,1)S(1)}, u32[]{:S(2)}, u32[]{:S(2)}) async-start(bf16[8,64,128]{2,1,0:T(8,128)(2,1)} %bitcast.6), calls=%async_computation | async-start | bytes 262144 | tf_op jit(solution)/shard_map/all_to_all | solution.py:50
  26.3 105.3 %all-gather.2.cloned.1.call-start = ((), (), s32[]{:S(2)}) async-start(), calls=%async_computation.4 | async-start | bytes 9437184 | tf_op jit(solution)/shard_map/all_gather | solution.py:73
  53.2 202.9 %reduce-scatter.2.cloned.1.call-start = ((), (), s32[]{:S(2)}) async-start(), calls=%async_computation.5 | async-start | bytes 9437184 | tf_op jit(solution)/shard_map/reduce_scatter | solution.py:87
  131.6 14.3 %copy-start.2 = (bf16[32,64,2048]{2,1,0:T(8,128)(2,1)S(1)}, bf16[32,64,2048]{2,1,0:T(8,128)(2,1)}, u32[]{:S(2)}) copy-start(bf16[32,64,2048]{2,1,0:T(8,128)(2,1)} %all-gather.2.cloned.1.call-done) | copy-start | bytes 25165828
  131.6 14.3 %copy-start.3 = (bf16[1,2048,896]{2,1,0:T(8,128)(2,1)S(1)}, bf16[1,2048,896]{2,1,0:T(8,128)(2,1)}, u32[]{:S(2)}) copy-start(bf16[1,2048,896]{2,1,0:T(8,128)(2,1)} %param.24) | copy-start | bytes 11010052
  145.9 11.3 %copy-start.4 = (bf16[1,896,2048]{2,1,0:T(8,128)(2,1)S(1)}, bf16[1,896,2048]{2,1,0:T(8,128)(2,1)}, u32[]{:S(2)}) copy-start(bf16[1,896,2048]{2,1,0:T(8,128)(2,1)} %param.25) | copy-start | bytes 11010052
  168.2 92.2 %copy-start = (s32[64,2]{0,1:T(2,128)S(1)}, s32[64,2]{0,1:T(2,128)}, u32[]{:S(2)}) copy-start(s32[64,2]{0,1:T(2,128)} %param.21) | copy-start | bytes 1540
  168.2 92.7 %copy-start.1 = (f32[64,2]{0,1:T(2,128)S(1)}, f32[64,2]{0,1:T(2,128)}, u32[]{:S(2)}) copy-start(f32[64,2]{0,1:T(2,128)} %param.22) | copy-start | bytes 1540
  256.0 18.4 %all-to-all-start.2 = ((bf16[4,64,2048]{2,1,0:T(8,128)(2,1)}), bf16[4,64,2048]{2,1,0:T(8,128)(2,1)S(1)}, u32[]{:S(2)}, u32[]{:S(2)}) async-start(bf16[4,64,2048]{2,1,0:T(8,128)(2,1)} %reduce-scatter.2.cloned.1.call-done), calls=%async_computation.3 | async-start | bytes 2097152 | tf_op jit(solution)/shard_map/all_to_all | solution.py:90
Sparse Core Ops, SparseCore 0:
  53.3 78.2 all-gather.1
  168.3 87.6 reduce-scatter.1
where the time goes:
time: 288 us; the launch traced here: 286 us
  waiting for transfers between devices  184 us (64%)
  matrix products  40.3 us (14%)
  blocking collectives  16.8 us (6%)
  starting transfers between devices  16.4 us (6%)
  between operations  13.6 us (5%)
  other arithmetic  9.52 us (3%)
  local copies, waits for them, and re-layouts  4.81 us (2%)
    reduce_scatter x1, waiting for transfers between devices, local(): lax.psum_scatter(partial_value.astype(jnp.bfloat16), 'tp', scatter_dimens...  87.8 us
    all_gather x1, waiting for transfers between devices, local(): lax.all_gather(lax.all_to_all(dispatch, 'sp', split_axis=0, concat_axis=0...  78.4 us
    all_to_all x1, blocking collectives, local(): lax.all_to_all(dispatch, 'sp', split_axis=0, concat_axis=0, tiled=True)  16.8 us
    dot_general x1, matrix products, local(): jnp.dot(flat_rows, w_gate[0], preferred_element_type=jnp.float32)  14.3 us
    all_to_all x1, waiting for transfers between devices, local(): lax.all_to_all(summed, 'sp', split_axis=0, concat_axis=0, tiled=True)  13.5 us
    dot_general x1, matrix products, local(): up_part = jnp.dot(flat_rows, w_up[0], preferred_element_type=jnp.float32)  11.3 us
    dot_general x1, matrix products, local(): jnp.dot(activated, w_down[0], preferred_element_type=jnp.float32)  11 us
    ppermute x2, starting transfers between devices, passed_along(): return lax.ppermute(block, axis, route)  6.79 us
  transfers between devices with their start and end apart: 6, of which 4 were waited for; matrix products, arithmetic and copies ran while one was open for 2% of the time, Pallas kernels for 0%

commit v1 on v0

--- a/solution.py
+++ b/solution.py
@@ -1,7 +1,333 @@
+import functools
+
 import jax
 import jax.numpy as jnp
 from jax import lax
+from jax.experimental import pallas as pl
+from jax.experimental.pallas import tpu as pltpu
 from jax.sharding import PartitionSpec as P
+
+MESH = pl.DeviceIdType.MESH
+LANES = 128
+
+
+def moe_kernel(
+    x_ref, wg_hbm, wu_hbm, wd_hbm, out_ref,
+    xbuf, pbuf, dbuf, r1, r2, rz, wg, wu, wd,
+    w_sem, own_sem,
+    s_z, r_z, s_1, s_2, r_h, s_p, r_p,
+    s_d, r_d, s_r1, r_r1, s_r2, r_r2, s_rz, r_rz,
+):
+    nz = lax.axis_size("tp") // 2
+    pairs = nz // 2
+    width = out_ref.shape[1]
+    half = width // 2
+    rows = out_ref.shape[0]
+    sp, tp = lax.axis_index("sp"), lax.axis_index("tp")
+    y, x = sp // 2, sp % 2
+    z, c = tp // 2, tp % 2
+    xn, yn, dg = y * 2 + 1 - x, (1 - y) * 2 + x, (1 - y) * 2 + 1 - x
+    other = (sp, z * 2 + 1 - c)
+    to_x, to_y = (xn, tp), (yn, tp)
+
+    def pair_of(q):
+        return (z // 2 + q) % pairs
+
+    def zz(k):
+        return 2 * pair_of(k // 2) + (z + k) % 2
+
+    def lanes(h):
+        return pl.ds(0, half) if h == 0 else pl.ds(half, xbuf.shape[3] - half)
+
+    def rc(src, dst, ss, rs, dev):
+        return pltpu.make_async_remote_copy(
+            src_ref=src, dst_ref=dst, send_sem=ss, recv_sem=rs,
+            device_id=dev, device_id_type=MESH,
+        )
+
+    def z_send(k):
+        return rc(x_ref, xbuf.at[sp * nz + z, c], s_z.at[k], r_z.at[z], (sp, zz(k) * 2 + c))
+
+    def z_recv(k):
+        return rc(x_ref, xbuf.at[sp * nz + zz(k), c], s_z.at[k], r_z.at[zz(k)], (sp, zz(k) * 2 + c))
+
+    def piece(h, col, k, ss, dev):
+        at = xbuf.at[col * nz + zz(k), c, :, lanes(h)]
+        return rc(at, at, ss, r_h.at[h, col * nz + zz(k)], dev)
+
+    def first(h, k):
+        return piece(h, sp, k, s_1.at[h, k], to_y if h == 0 else to_x)
+
+    def second(h, k):
+        return piece(h, sp, k, s_2.at[h, 0, k], to_x if h == 0 else to_y)
+
+    def third(h, k):
+        return piece(h, yn if h == 0 else xn, k, s_2.at[h, 1, k], to_x if h == 0 else to_y)
+
+    def arrived(h, col, k):
+        piece(h, col, k, s_1.at[h, k], other).wait_recv()
+
+    def to_other(col, k):
+        i = col * nz + zz(k)
+        return rc(xbuf.at[i, c], xbuf.at[i, c], s_p.at[i], r_p.at[i], other)
+
+    def from_other(i):
+        rc(xbuf.at[i, 1 - c], xbuf.at[i, 1 - c], s_p.at[i], r_p.at[i], other).wait_recv()
+
+    def spread(k):
+        for h in (1, 0):
+            first(h, k).start()
+        for h in (0, 1):
+            second(h, k).start()
+        to_other(sp, k).start()
+
+    def take_z(k):
+        z_recv(k).wait_recv()
+        spread(k)
+
+    def relay(q):
+        for k in (2 * q, 2 * q + 1):
+            arrived(0, yn, k)
+            third(0, k).start()
+            arrived(1, xn, k)
+            third(1, k).start()
+
+    def sides(q):
+        for k in (2 * q, 2 * q + 1):
+            arrived(0, xn, k)
+            to_other(xn, k).start()
+            arrived(1, yn, k)
+            to_other(yn, k).start()
+
+    def corner(q):
+        for k in (2 * q, 2 * q + 1):
+            arrived(0, dg, k)
+            arrived(1, dg, k)
+            to_other(dg, k).start()
+
+    def d_copy(col, p, mine):
+        i = pl.ds(col * nz + 2 * p, 2)
+        at = pbuf.at[i, 1 - c]
+        return rc(at, dbuf.at[i], s_d.at[col * pairs + p], r_d.at[col * pairs + p], other)
+
+    def cols(h):
+        return pl.ds(h * half, half)
+
+    def r1_copy(h, o, p):
+        col = dg if o else (xn if h == 0 else yn)
+        at = pbuf.at[pl.ds(col * nz + 2 * p, 2), c, :, cols(h)]
+        return rc(at, r1.at[h, o, pl.ds(2 * p, 2)], s_r1.at[h, o, p], r_r1.at[h, o, p], to_x if h == 0 else to_y)
+
+    def r2_copy(h, p):
+        col = yn if h == 0 else xn
+        at = pbuf.at[pl.ds(col * nz + 2 * p, 2), c, :, cols(h)]
+        return rc(at, r2.at[h, pl.ds(2 * p, 2)], s_r2.at[h, p], r_r2.at[h, p], to_y if h == 0 else to_x)
+
+    def rz_copy(k):
+        return rc(pbuf.at[sp * nz + zz(k), c], rz.at[z], s_rz.at[k], r_rz.at[z], (sp, zz(k) * 2 + c))
+
+    def rz_recv(k):
+        return rc(pbuf.at[sp * nz + zz(k), c], rz.at[zz(k)], s_rz.at[k], r_rz.at[zz(k)], (sp, zz(k) * 2 + c))
+
+    f32 = jnp.float32
+
+    def merge(fy, fx, p):
+        col = (y + fy - 2 * y * fy) * 2 + x + fx - 2 * x * fx
+        d_copy(col, p, False).wait_recv()
+        i = pl.ds(col * nz + 2 * p, 2)
+        pbuf[i, c] = (pbuf[i, c].astype(f32) + dbuf[i].astype(f32)).astype(pbuf.dtype)
+
+    def send_sum(g, p):
+        @pl.when(g == 1)
+        def _():
+            r1_copy(0, 0, p).start()
+
+        @pl.when(g == 2)
+        def _():
+            r1_copy(1, 0, p).start()
+
+        @pl.when(g == 3)
+        def _():
+            r1_copy(0, 1, p).start()
+            r1_copy(1, 1, p).start()
+
+    def stage2(q):
+        p = pair_of(q)
+        for h in (0, 1):
+            r1_copy(h, 1, p).wait_recv()
+            col = yn if h == 0 else xn
+            i = pl.ds(col * nz + 2 * p, 2)
+            pbuf[i, c, :, cols(h)] = (
+                pbuf[i, c, :, cols(h)].astype(f32) + r1[h, 1, pl.ds(2 * p, 2)].astype(f32)
+            ).astype(pbuf.dtype)
+            r2_copy(h, p).start()
+
+    def stage3(q):
+        p = pair_of(q)
+        i = pl.ds(sp * nz + 2 * p, 2)
+        j = pl.ds(2 * p, 2)
+        for h in (0, 1):
+            r1_copy(h, 0, p).wait_recv()
+            r2_copy(h, p).wait_recv()
+            pbuf[i, c, :, cols(h)] = (
+                pbuf[i, c, :, cols(h)].astype(f32)
+                + r1[h, 0, j].astype(f32)
+                + r2[h, j].astype(f32)
+            ).astype(pbuf.dtype)
+        for k in (2 * q, 2 * q + 1):
+            if k > 0:
+                rz_copy(k).start()
+
+    weights = [
+        pltpu.make_async_copy(a, b, w_sem.at[n])
+        for n, (a, b) in enumerate(((wg_hbm, wg), (wu_hbm, wu), (wd_hbm, wd)))
+    ]
+    own = pltpu.make_async_copy(x_ref, xbuf.at[sp * nz + z, c], own_sem)
+    own.start()
+    barrier = pltpu.get_barrier_semaphore()
+    peers = [other, to_x, to_y] + [(sp, zz(k) * 2 + c) for k in range(1, nz)]
+    for peer in peers:
+        pl.semaphore_signal(barrier, inc=1, device_id=peer, device_id_type=MESH)
+    pl.semaphore_wait(barrier, len(peers))
+    for k in range(1, nz):
+        z_send(k).start()
+    own.wait()
+    spread(0)
+    for w in weights:
+        w.start()
+    take_z(1)
+    for w in weights:
+        w.wait()
+
+    experts_lanes = lax.axis_size("sp")
+    lane = lax.broadcasted_iota(jnp.int32, (1, LANES), 1)
+    mine = ((lane % experts_lanes == sp) & (lane < 3 * experts_lanes)).astype(f32)
+
+    before = {1: [lambda: relay(0), lambda: sides(0)]}
+    for q in range(1, pairs):
+        base = 4 * (q - 1)
+        before.setdefault(base + 2, []).append(functools.partial(take_z, 2 * q))
+        before.setdefault(base + 3, []).append(functools.partial(take_z, 2 * q + 1))
+        before.setdefault(4 * q + 1, []).append(functools.partial(relay, q))
+        before.setdefault(4 * q + 1, []).append(functools.partial(sides, q))
+    for q in range(pairs):
+        before.setdefault(4 * q + 3, []).append(functools.partial(corner, q))
+    after = {}
+    for q in range(pairs - 1):
+        after.setdefault(4 * q + 6, []).append(functools.partial(stage2, q))
+
+    @pl.loop(0, 4 * pairs)
+    def _(s):
+        for at, works in before.items():
+            @pl.when(s == at)
+            def _():
+                for work in works:
+                    work()
+
+        g = s % 4
+        fy, fx = g // 2, g % 2
+        p = pair_of(s // 4)
+        col = (y + fy - 2 * y * fy) * 2 + x + fx - 2 * x * fx
+        i = col * nz + 2 * p
+        for b in (0, 1):
+            from_other(i + b)
+        held = xbuf[pl.ds(i, 2)].reshape(4 * rows, xbuf.shape[3])
+        scale = jnp.sum(held[:, width:].astype(f32) * mine, axis=1, keepdims=True)
+        held = held[:, :width]
+        gate = jnp.dot(held, wg[...], preferred_element_type=f32)
+        up = jnp.dot(held, wu[...], preferred_element_type=f32)
+        act = (jax.nn.silu(gate) * up * scale).astype(jnp.bfloat16)
+        part = jnp.dot(act, wd[...], preferred_element_type=f32)
+        pbuf[pl.ds(i, 2)] = part.astype(pbuf.dtype).reshape(2, 2, rows, width)
+        d_copy(col, p, True).start()
+
+        @pl.when(s > 0)
+        def _():
+            t = s - 1
+            gt = t % 4
+            pt = pair_of(t // 4)
+            merge(gt // 2, gt % 2, pt)
+            send_sum(gt, pt)
+
+        for at, works in after.items():
+            @pl.when(s == at)
+            def _():
+                for work in works:
+                    work()
+
+    last = pair_of(pairs - 1)
+    merge(1, 1, last)
+    send_sum(3, last)
+    for q in range(pairs - 1):
+        stage3(q)
+    stage2(pairs - 1)
+    stage3(pairs - 1)
+    total = pbuf[sp * nz + z, c].astype(f32)
+    for k in range(1, nz):
+        rz_recv(k).wait_recv()
+        total = total + rz[zz(k)].astype(f32)
+    out_ref[...] = total
+
+    for k in range(1, nz):
+        z_send(k).wait_send()
+        rz_copy(k).wait_send()
+    for k in range(nz):
+        for h in (0, 1):
+            first(h, k).wait_send()
+            second(h, k).wait_send()
+            third(h, k).wait_send()
+        for col in (sp, xn, yn, dg):
+            to_other(col, k).wait_send()
+    for q in range(pairs):
+        p = pair_of(q)
+        for col in (sp, xn, yn, dg):
+            d_copy(col, p, True).wait_send()
+        for h in (0, 1):
+            for o in (0, 1):
+                r1_copy(h, o, p).wait_send()
+            r2_copy(h, p).wait_send()
+
+
+def moe(x_ext, w_gate, w_up, w_down):
+    rows = x_ext.shape[0]
+    wide = x_ext.shape[1]
+    width = w_down.shape[1]
+    n_sp = lax.axis_size("sp")
+    nz = lax.axis_size("tp") // 2
+    pairs = nz // 2
+    half = width // 2
+    bf = jnp.bfloat16
+    dma = pltpu.SemaphoreType.DMA
+    hbm = pl.BlockSpec(memory_space=pl.ANY)
+    vmem = pl.BlockSpec(memory_space=pltpu.VMEM)
+    return pl.pallas_call(
+        moe_kernel,
+        out_shape=jax.ShapeDtypeStruct((rows, width), jnp.float32),
+        in_specs=[vmem, hbm, hbm, hbm],
+        out_specs=vmem,
+        scratch_shapes=[
+            pltpu.VMEM((n_sp * nz, 2, rows, wide), bf),
+            pltpu.VMEM((n_sp * nz, 2, rows, width), bf),
+            pltpu.VMEM((n_sp * nz, rows, width), bf),
+            pltpu.VMEM((2, 2, nz, rows, half), bf),
+            pltpu.VMEM((2, nz, rows, half), bf),
+            pltpu.VMEM((nz, rows, width), bf),
+            pltpu.VMEM(w_gate.shape, bf),
+            pltpu.VMEM(w_up.shape, bf),
+            pltpu.VMEM(w_down.shape, bf),
+            dma((3,)), dma,
+            dma((nz,)), dma((nz,)),
+            dma((2, nz)), dma((2, 2, nz)), dma((2, n_sp * nz)),
+            dma((n_sp * nz,)), dma((n_sp * nz,)),
+            dma((n_sp * pairs,)), dma((n_sp * pairs,)),
+            dma((2, 2, pairs)), dma((2, 2, pairs)),
+            dma((2, pairs)), dma((2, pairs)),
+            dma((nz,)), dma((nz,)),
+        ],
+        compiler_params=pltpu.CompilerParams(
+            collective_id=0, has_side_effects=True, vmem_limit_bytes=64000000
+        ),
+    )(x_ext, w_gate, w_up, w_down)
 
 
 def passed_along(block, axis, distance):
@@ -58,6 +384,18 @@
     ).astype(jnp.bfloat16)
     experts = lax.axis_size("sp") * w_gate.shape[0]
     capacity = 4 * local_rows // experts
+    if lax.axis_size("sp") == 4 and w_gate.shape[0] == 1 and capacity >= local_rows:
+        named = route_ids[:, :, None] == jnp.arange(experts, dtype=jnp.int32)[None, None, :]
+        share = jnp.sum(jnp.where(named, route_weight[:, :, None], 0.0), axis=1)
+        high = lax.reduce_precision(share, 8, 7)
+        middle = lax.reduce_precision(share - high, 8, 7)
+        low = share - high - middle
+        spare = jnp.zeros((local_rows, LANES - 3 * experts), jnp.float32)
+        shares = jnp.concatenate([high, middle, low, spare], axis=1).astype(jnp.bfloat16)
+        combined = moe(
+            jnp.concatenate([normed, shares], axis=1), w_gate[0], w_up[0], w_down[0]
+        )
+        return (hidden_state.astype(jnp.float32) + combined).astype(jnp.bfloat16)
     flat_ids = route_ids.reshape(-1)
     one_hot = (flat_ids[:, None] == jnp.arange(experts, dtype=jnp.int32)[None, :]).astype(jnp.int32)
     rank_in = jnp.sum((jnp.cumsum(one_hot, axis=0) - one_hot) * one_hot, axis=1)

time: 288 us -> 137 us (0.48)
  waiting for transfers between devices: 184 us -> 4.63 us
  Pallas kernels: 0 us -> 106 us
  matrix products: 40.3 us -> 3.17 us
  blocking collectives: 16.8 us -> 0 us
  between operations: 13.6 us -> 0.07 us
  starting transfers between devices: 16.4 us -> 12.1 us
    pallas_call x0 -> x1, Pallas kernels: none -> 106 us  [moe(): pl.pallas_call(moe_kernel, out_shape=jax.ShapeDtypeStruct((rows, width),...]
    reduce_scatter x1 -> x0, waiting for transfers between devices: 87.8 us -> none  [local(): lax.psum_scatter(partial_value.astype(jnp.bfloat16), 'tp', scatter_dimens...]
    all_gather x1 -> x0, waiting for transfers between devices: 78.4 us -> none  [local(): lax.all_gather(lax.all_to_all(dispatch, 'sp', split_axis=0, concat_axis=0...]
    dot_general x4 -> x0, matrix products: 37.1 us -> none  [the longest x1 14.3 us: local(): jnp.dot(flat_rows, w_gate[0], preferred_element_type=jnp.float32)]
    all_to_all x1 -> x0, blocking collectives: 16.8 us -> none  [local(): lax.all_to_all(dispatch, 'sp', split_axis=0, concat_axis=0, tiled=True)]
    all_to_all x1 -> x0, waiting for transfers between devices: 13.5 us -> none  [local(): lax.all_to_all(summed, 'sp', split_axis=0, concat_axis=0, tiled=True)]
    all_to_all x1 -> x0, starting transfers between devices: 4.2 us -> none  [local(): lax.all_to_all(summed, 'sp', split_axis=0, concat_axis=0, tiled=True)]
  transfers between devices with their start and end apart: 6 -> 3, of which waited for: 4 -> 1; matrix products, arithmetic and copies ran while one was open for 2% -> 4% of each run, Pallas kernels for 0% -> 0%
where the time goes in v1:
time: 137 us
  Pallas kernels  106 us (77%)
  starting transfers between devices  12.1 us (9%)
  other arithmetic  8.34 us (6%)
  waiting for transfers between devices  4.63 us (3%)
  matrix products  3.17 us (2%)
  local copies, waits for them, and re-layouts  2.58 us (2%)
    pallas_call x1, Pallas kernels, moe(): pl.pallas_call(moe_kernel, out_shape=jax.ShapeDtypeStruct((rows, width),...  106 us
    ppermute x2, starting transfers between devices, passed_along(): return lax.ppermute(block, axis, route)  6.79 us
    all_to_all x1, starting transfers between devices, local(): lax.all_to_all(mixed_rows, 'tp', split_axis=0, concat_axis=1, tiled=True)  5.32 us
    all_to_all x1, waiting for transfers between devices, local(): lax.all_to_all(mixed_rows, 'tp', split_axis=0, concat_axis=1, tiled=True)  4.63 us
    dot_general x1, matrix products, local(): projected = jnp.dot(token_rows, w_out, preferred_element_type=jnp.float32)  3.17 us
  transfers between devices with their start and end apart: 3, of which 1 were waited for; matrix products, arithmetic and copies ran while one was open for 4% of the time, Pallas kernels for 0%

profile of v1, /device:TPU:10, one launch (start us, length us, event | category | flops | bytes accessed | tf_op | source)
XLA Modules:
  0.0 136.8 jit_solution(17966663198172562175)
XLA Ops:
  0.0 0.8 slice.43
  0.8 3.4 %collective-permute-start.1 = (s32[2]{0:T(128)S(1)}, s32[2]{0:T(128)S(1)}, u32[]{:S(2)}, u32[]{:S(2)}) collective-permute-start(s32[2]{0:T(128)S(1)} %slice.43), channel_id=1, source_target_pairs={{0,8},{8,16},{16,24},{1,9},{9,17},{17,25},{2,10},{10,18},{18,26},{... | collective-permute-start | bytes 32 | tf_op jit(solution)/shard_map/ppermute | solution.py:336
  4.1 0.7 slice_bitcast_fusion.1
  4.9 3.4 %collective-permute-start = (bf16[2,2,128]{2,1,0:T(2,128)(2,1)S(1)}, bf16[2,2,128]{2,1,0:T(2,128)(2,1)S(1)}, u32[]{:S(2)}, u32[]{:S(2)}) collective-permute-start(bf16[2,2,128]{2,1,0:T(2,128)(2,1)S(1)} %pad_maximum_fusion.1), channel_id=1, source_target_pairs={{0,8},{8,16},{16,24},{1,9},{9,17},{17,25},{2,10},{10,18},{18,26},{... | collective-permute-start | bytes 3080 | tf_op jit(solution)/shard_map/ppermute | solution.py:336
  8.3 1.0 convert_multiply_fusion
  9.3 0.7 convert_element_type.51
  10.0 0.7 select_reduce_fusion
  10.7 0.0 collective-permute-done.1
  10.7 0.8 pad_add_fusion
  11.4 0.8 fusion.14
  12.2 0.0 collective-permute-done
  12.2 1.8 %fusion.8 = bf16[512,128]{1,0:T(8,128)(2,1)} fusion(f32[2,128]{1,0:T(2,128)S(1)} %multiply_bitcast_fusion, f32[512,128]{1,0:T(8,128)S(1)} %convert_multiply_fusion, bf16[512,128]{1,0:T(8,128)(2,1)} %param.13, f32[512]{0:T(512)S(1)} %get-tuple-element.8, f32[128]{0:T(128)S(1)} %get-tuple-element.12, f32[512]{0:T(512)S(1)} %get-tuple-element.7, ...), kind=kLoop, calls=%fused_computation.14 | loop fusion | flops 786432 | bytes 530944 | tf_op jit(solution)/shard_map/convert_element_type | solution.py:375
  14.0 5.3 %all-to-all-start = ((bf16[8,64,128]{2,1,0:T(8,128)(2,1)}), bf16[8,64,128]{2,1,0:T(8,128)(2,1)S(1)}, u32[]{:S(2)}, u32[]{:S(2)}) async-start(bf16[8,64,128]{2,1,0:T(8,128)(2,1)} %bitcast.6), calls=%async_computation | async-start | bytes 262144 | tf_op jit(solution)/shard_map/all_to_all | solution.py:376
  19.3 0.1 copy.26
  19.4 0.7 convert_element_type.61
  20.1 0.1 copy.28
  20.2 0.1 copy.27
  20.3 4.6 %all-to-all-done = bf16[8,64,128]{2,1,0:T(8,128)(2,1)S(1)} async-done(((bf16[8,64,128]{2,1,0:T(8,128)(2,1)}), bf16[8,64,128]{2,1,0:T(8,128)(2,1)S(1)}, u32[]{:S(2)}, u32[]{:S(2)}) %all-to-all-start) | async-done | bytes 131104 | tf_op jit(solution)/shard_map/all_to_all | solution.py:376
  24.9 3.2 %multiply_reduce_fusion = (f32[64]{0:T(128)S(1)}, f32[64,2048]{1,0:T(8,128)S(1)}) fusion(bf16[1024,2048]{1,0:T(8,128)(2,1)} %param.18, bf16[64,2048]{1,0:T(8,128)(2,1)} %param.19, bf16[8,64,128]{2,1,0:T(8,128)(2,1)S(1)} %all-to-all-done), kind=kOutput, calls=%fused_computation.5 | convolution fusion | flops 269221824 | bytes 5112064 | tf_op jit(solution)/shard_map/dot_general | solution.py:377
  28.1 0.1 multiply_convert_fusion
  28.3 0.8 concatenate.14.x_ref
  29.1 105.9 %shard_map.127 = f32[64,2048]{1,0:T(8,128)} custom-call(bf16[64,2176]{1,0:T(8,128)(2,1)} %concatenate.14.x_ref, bf16[2048,896]{1,0:T(8,128)(2,1)} %bitcast.27, bf16[2048,896]{1,0:T(8,128)(2,1)} %bitcast.28, bf16[896,2048]{1,0:T(8,128)(2,1)} %bitcast.29), custom_call_target="tpu_custom_call" | custom-call | tf_op jit(solution)/shard_map/pallas_call | solution.py:303
  135.0 1.8 %add_convert_fusion = bf16[64,2048]{1,0:T(8,128)(2,1)} fusion(f32[64,2048]{1,0:T(8,128)S(1)} %get-tuple-element.15, f32[64,2048]{1,0:T(8,128)} %shard_map.127), kind=kLoop, calls=%fused_computation.3 | loop fusion | flops 262144 | bytes 1310720 | tf_op jit(solution)/shard_map/convert_element_type | solution.py:398
  (7 shorter events, 0.0 us)
Async XLA Ops:
  0.8 9.9 %collective-permute-start.1 = (s32[2]{0:T(128)S(1)}, s32[2]{0:T(128)S(1)}, u32[]{:S(2)}, u32[]{:S(2)}) collective-permute-start(s32[2]{0:T(128)S(1)} %slice.43), channel_id=1, source_target_pairs={{0,8},{8,16},{16,24},{1,9},{9,17},{17,25},{2,10},{10,18},{18,26},{... | collective-permute-start | bytes 32 | tf_op jit(solution)/shard_map/ppermute | solution.py:336
  4.9 7.3 %collective-permute-start = (bf16[2,2,128]{2,1,0:T(2,128)(2,1)S(1)}, bf16[2,2,128]{2,1,0:T(2,128)(2,1)S(1)}, u32[]{:S(2)}, u32[]{:S(2)}) collective-permute-start(bf16[2,2,128]{2,1,0:T(2,128)(2,1)S(1)} %pad_maximum_fusion.1), channel_id=1, source_target_pairs={{0,8},{8,16},{16,24},{1,9},{9,17},{17,25},{2,10},{10,18},{18,26},{... | collective-permute-start | bytes 3080 | tf_op jit(solution)/shard_map/ppermute | solution.py:336
  14.0 11.0 %all-to-all-start = ((bf16[8,64,128]{2,1,0:T(8,128)(2,1)}), bf16[8,64,128]{2,1,0:T(8,128)(2,1)S(1)}, u32[]{:S(2)}, u32[]{:S(2)}) async-start(bf16[8,64,128]{2,1,0:T(8,128)(2,1)} %bitcast.6), calls=%async_computation | async-start | bytes 262144 | tf_op jit(solution)/shard_map/all_to_all | solution.py:376

commit v2 on v1

--- a/solution.py
+++ b/solution.py
@@ -12,7 +12,9 @@
 
 
 def moe_kernel(
-    x_ref, wg_hbm, wu_hbm, wd_hbm, out_ref,
+    gb, gc, vals, taps, docs, resid, gain, ids, route, wo_hbm, wg_hbm, wu_hbm, wd_hbm, out_ref,
+    x_ref, hid, tok, mixed, pad, dpad, hc, hv, hd, wo,
+    s_a, r_a, s_h, r_h3,
     xbuf, pbuf, dbuf, r1, r2, rz, wg, wu, wd,
     w_sem, own_sem,
     s_z, r_z, s_1, s_2, r_h, s_p, r_p,
@@ -28,6 +30,10 @@
     z, c = tp // 2, tp % 2
     xn, yn, dg = y * 2 + 1 - x, (1 - y) * 2 + x, (1 - y) * 2 + 1 - x
     other = (sp, z * 2 + 1 - c)
+    n_sp, n_tp = lax.axis_size("sp"), lax.axis_size("tp")
+    following, previous = (lax.rem(sp + 1, n_sp), tp), (lax.rem(sp + n_sp - 1, n_sp), tp)
+    seq = gb.shape[0]
+    halo = hc.shape[0]
     to_x, to_y = (xn, tp), (yn, tp)
 
     def pair_of(q):
@@ -44,6 +50,68 @@
             src_ref=src, dst_ref=dst, send_sem=ss, recv_sem=rs,
             device_id=dev, device_id_type=MESH,
         )
+
+    def halo_copies():
+        pairs3 = ((gc.at[pl.ds(seq - halo, halo)], hc), (vals.at[pl.ds(seq - halo, halo)], hv),
+                  (docs.at[pl.ds(seq - 8, 8)], hd))
+        return [rc(a, b, s_h.at[n], r_h3.at[n], following) for n, (a, b) in enumerate(pairs3)]
+
+    def channels(j):
+        return pl.ds(pl.multiple_of(j * gb.shape[1], gb.shape[1]), gb.shape[1])
+
+    def swap(d):
+        j = lax.rem(tp + d, n_tp)
+        at = mixed.at[pl.ds(pl.multiple_of(j * rows, rows), rows)]
+        return rc(at, tok.at[:, channels(tp)], s_a.at[d], r_a.at[tp], (sp, j))
+
+    def swapped(d):
+        j = lax.rem(tp + d, n_tp)
+        at = mixed.at[pl.ds(pl.multiple_of(j * rows, rows), rows)]
+        return rc(at, tok.at[:, channels(j)], s_a.at[d], r_a.at[j], (sp, j))
+
+    def mix():
+        f32 = jnp.float32
+        product = gc[...].astype(f32) * vals[...].astype(f32)
+        pad[pl.ds(8, seq)] = product
+        dpad[pl.ds(8, seq)] = docs[...]
+        for copy in halo_copies():
+            copy.wait_recv()
+        pad[pl.ds(0, 8)] = (hc[...].astype(f32) * hv[...].astype(f32))[halo - 8 :]
+        dpad[pl.ds(0, 8)] = jnp.where(sp == 0, -1, hd[...])
+        near = (dpad[pl.ds(7, seq)] == docs[...]).astype(f32)
+        far = (dpad[pl.ds(6, seq)] == docs[...]).astype(f32)
+        tap = taps[...].astype(f32)
+        convolved = (
+            tap[2:3] * product
+            + tap[1:2] * pad[pl.ds(7, seq)] * near
+            + tap[0:1] * pad[pl.ds(6, seq)] * far
+        )
+        mixed[...] = (gb[...].astype(f32) * convolved).astype(mixed.dtype)
+        for d in range(1, n_tp):
+            swap(d).start()
+        tok[:, channels(tp)] = mixed[pl.ds(pl.multiple_of(tp * rows, rows), rows)]
+        lane = lax.broadcasted_iota(jnp.int32, (rows, LANES), 1)
+        named = lane % n_sp
+        part = lane // n_sp
+        share = jnp.where(ids[:, 0:1] == named, route[:, 0:1], 0.0) + jnp.where(
+            ids[:, 1:2] == named, route[:, 1:2], 0.0
+        )
+        high = share.astype(jnp.bfloat16).astype(f32)
+        middle = (share - high).astype(jnp.bfloat16).astype(f32)
+        low = share - high - middle
+        terms = jnp.where(part == 0, high, jnp.where(part == 1, middle, jnp.where(part == 2, low, 0.0)))
+        x_ref[:, pl.ds(width, LANES)] = terms.astype(x_ref.dtype)
+        wo_copy.wait()
+        for d in range(1, n_tp):
+            swapped(d).wait_recv()
+        projected = jnp.dot(tok[...], wo[...], preferred_element_type=f32)
+        hidden = (resid[...].astype(f32) + projected).astype(hid.dtype)
+        hid[...] = hidden
+        state = hidden.astype(f32)
+        mean = jnp.mean(state * state, axis=-1, keepdims=True)
+        x_ref[:, pl.ds(0, width)] = (
+            state * lax.rsqrt(mean + 1e-06) * gain[...].astype(f32)
+        ).astype(x_ref.dtype)
 
     def z_send(k):
         return rc(x_ref, xbuf.at[sp * nz + z, c], s_z.at[k], r_z.at[z], (sp, zz(k) * 2 + c))
@@ -183,18 +251,23 @@
         for n, (a, b) in enumerate(((wg_hbm, wg), (wu_hbm, wu), (wd_hbm, wd)))
     ]
     own = pltpu.make_async_copy(x_ref, xbuf.at[sp * nz + z, c], own_sem)
-    own.start()
+    wo_copy = pltpu.make_async_copy(wo_hbm, wo, w_sem.at[3])
+    wo_copy.start()
+    for w in weights:
+        w.start()
     barrier = pltpu.get_barrier_semaphore()
-    peers = [other, to_x, to_y] + [(sp, zz(k) * 2 + c) for k in range(1, nz)]
+    peers = [to_x, to_y, following, previous] + [(sp, lax.rem(tp + d, n_tp)) for d in range(1, n_tp)]
     for peer in peers:
         pl.semaphore_signal(barrier, inc=1, device_id=peer, device_id_type=MESH)
     pl.semaphore_wait(barrier, len(peers))
+    for copy in halo_copies():
+        copy.start()
+    mix()
+    own.start()
     for k in range(1, nz):
         z_send(k).start()
     own.wait()
     spread(0)
-    for w in weights:
-        w.start()
     take_z(1)
     for w in weights:
         w.wait()
@@ -266,8 +339,12 @@
     for k in range(1, nz):
         rz_recv(k).wait_recv()
         total = total + rz[zz(k)].astype(f32)
-    out_ref[...] = total
-
+    out_ref[...] = (hid[...].astype(f32) + total).astype(out_ref.dtype)
+
+    for copy in halo_copies():
+        copy.wait_send()
+    for d in range(1, n_tp):
+        swap(d).wait_send()
     for k in range(1, nz):
         z_send(k).wait_send()
         rz_copy(k).wait_send()
@@ -288,10 +365,11 @@
             r2_copy(h, p).wait_send()
 
 
-def moe(x_ext, w_gate, w_up, w_down):
-    rows = x_ext.shape[0]
-    wide = x_ext.shape[1]
-    width = w_down.shape[1]
+def layer(gate_b, gate_c, values_in, conv_w, docs, resid, gain, ids, route, w_out, w_gate, w_up, w_down):
+    rows, width = resid.shape
+    wide = width + LANES
+    seq, held = gate_b.shape
+    n_tp = lax.axis_size("tp")
     n_sp = lax.axis_size("sp")
     nz = lax.axis_size("tp") // 2
     pairs = nz // 2
@@ -302,10 +380,21 @@
     vmem = pl.BlockSpec(memory_space=pltpu.VMEM)
     return pl.pallas_call(
         moe_kernel,
-        out_shape=jax.ShapeDtypeStruct((rows, width), jnp.float32),
-        in_specs=[vmem, hbm, hbm, hbm],
+        out_shape=jax.ShapeDtypeStruct((rows, width), bf),
+        in_specs=[vmem] * 9 + [hbm] * 4,
         out_specs=vmem,
         scratch_shapes=[
+            pltpu.VMEM((rows, wide), bf),
+            pltpu.VMEM((rows, width), bf),
+            pltpu.VMEM((rows, n_tp * held), bf),
+            pltpu.VMEM((seq, held), bf),
+            pltpu.VMEM((seq + 8, held), jnp.float32),
+            pltpu.VMEM((seq + 8, held), jnp.int32),
+            pltpu.VMEM((16, held), bf),
+            pltpu.VMEM((16, held), bf),
+            pltpu.VMEM((8, held), jnp.int32),
+            pltpu.VMEM(w_out.shape, bf),
+            dma((n_tp,)), dma((n_tp,)), dma((3,)), dma((3,)),
             pltpu.VMEM((n_sp * nz, 2, rows, wide), bf),
             pltpu.VMEM((n_sp * nz, 2, rows, width), bf),
             pltpu.VMEM((n_sp * nz, rows, width), bf),
@@ -315,7 +404,7 @@
             pltpu.VMEM(w_gate.shape, bf),
             pltpu.VMEM(w_up.shape, bf),
             pltpu.VMEM(w_down.shape, bf),
-            dma((3,)), dma,
+            dma((4,)), dma,
             dma((nz,)), dma((nz,)),
             dma((2, nz)), dma((2, 2, nz)), dma((2, n_sp * nz)),
             dma((n_sp * nz,)), dma((n_sp * nz,)),
@@ -327,7 +416,7 @@
         compiler_params=pltpu.CompilerParams(
             collective_id=0, has_side_effects=True, vmem_limit_bytes=64000000
         ),
-    )(x_ext, w_gate, w_up, w_down)
+    )(gate_b, gate_c, values_in, conv_w, docs, resid, gain, ids, route, w_out, w_gate, w_up, w_down)
 
 
 def passed_along(block, axis, distance):
@@ -354,6 +443,14 @@
     seq_rows = gate_b.shape[0]
     local_rows = resid.shape[0]
     model_width = resid.shape[1]
+    experts = lax.axis_size("sp") * w_gate.shape[0]
+    capacity = 4 * local_rows // experts
+    if lax.axis_size("sp") == 4 and w_gate.shape[0] == 1 and capacity >= local_rows:
+        docs = jnp.broadcast_to(documents[:, None], gate_b.shape)
+        return layer(
+            gate_b, gate_c, values_in, conv_w, docs, resid, norm_gain[None, :], route_ids,
+            route_weight, w_out, w_gate[0], w_up[0], w_down[0],
+        )
     last_rows = jnp.stack([gate_c[seq_rows - 2 :], values_in[seq_rows - 2 :]])
     before, before_docs = passed_along((last_rows, documents[seq_rows - 2 :]), "sp", 1)
     products = jnp.concatenate(
@@ -384,18 +481,6 @@
     ).astype(jnp.bfloat16)
     experts = lax.axis_size("sp") * w_gate.shape[0]
     capacity = 4 * local_rows // experts
-    if lax.axis_size("sp") == 4 and w_gate.shape[0] == 1 and capacity >= local_rows:
-        named = route_ids[:, :, None] == jnp.arange(experts, dtype=jnp.int32)[None, None, :]
-        share = jnp.sum(jnp.where(named, route_weight[:, :, None], 0.0), axis=1)
-        high = lax.reduce_precision(share, 8, 7)
-        middle = lax.reduce_precision(share - high, 8, 7)
-        low = share - high - middle
-        spare = jnp.zeros((local_rows, LANES - 3 * experts), jnp.float32)
-        shares = jnp.concatenate([high, middle, low, spare], axis=1).astype(jnp.bfloat16)
-        combined = moe(
-            jnp.concatenate([normed, shares], axis=1), w_gate[0], w_up[0], w_down[0]
-        )
-        return (hidden_state.astype(jnp.float32) + combined).astype(jnp.bfloat16)
     flat_ids = route_ids.reshape(-1)
     one_hot = (flat_ids[:, None] == jnp.arange(experts, dtype=jnp.int32)[None, :]).astype(jnp.int32)
     rank_in = jnp.sum((jnp.cumsum(one_hot, axis=0) - one_hot) * one_hot, axis=1)

time: 137 us -> 125 us (0.912)
  starting transfers between devices: 12.1 us -> 0 us
  Pallas kernels: 106 us -> 117 us
  other arithmetic: 8.34 us -> 0 us
  waiting for transfers between devices: 4.63 us -> 0 us
  local copies, waits for them, and re-layouts: 2.58 us -> 7.2 us
  matrix products: 3.17 us -> 0 us
    pallas_call x1, Pallas kernels: 106 us -> 117 us  [layer(): pl.pallas_call(moe_kernel, out_shape=jax.ShapeDtypeStruct((rows, width),...]
    ppermute x2 -> x0, starting transfers between devices: 6.79 us -> none  [passed_along(): return lax.ppermute(block, axis, route)]
    convert_element_type x6 -> x0, other arithmetic: 5.84 us -> none  [the longest x1 1.82 us: local(): return (hidden_state.astype(jnp.float32) + combined).astype(jnp.bfloat16)]
    all_to_all x1 -> x0, starting transfers between devices: 5.32 us -> none  [local(): lax.all_to_all(mixed_rows, 'tp', split_axis=0, concat_axis=1, tiled=True)]
    all_to_all x1 -> x0, waiting for transfers between devices: 4.63 us -> none  [local(): lax.all_to_all(mixed_rows, 'tp', split_axis=0, concat_axis=1, tiled=True)]
    unnamed x0 -> x3, local copies, waits for them, and re-layouts: none -> 4.4 us
    dot_general x1 -> x0, matrix products: 3.17 us -> none  [local(): projected = jnp.dot(token_rows, w_out, preferred_element_type=jnp.float32)]
    broadcast_in_dim x1 -> x2, local copies, waits for them, and re-layouts: 0.01 us -> 2.8 us  [the longest x1 1.52 us: local(): docs = jnp.broadcast_to(documents[:, None], gate_b.shape)]
  transfers between devices with their start and end apart: 3 -> 0, of which waited for: 1 -> 0; matrix products, arithmetic and copies ran while one was open for 4% -> 0% of each run, Pallas kernels for 0% -> 0%
where the time goes in v2:
time: 125 us; the launch traced here: 124 us
  Pallas kernels  117 us (94%)
  local copies, waits for them, and re-layouts  7.2 us (6%)
    pallas_call x1, Pallas kernels, layer(): pl.pallas_call(moe_kernel, out_shape=jax.ShapeDtypeStruct((rows, width),...  117 us
    unnamed x3, local copies, waits for them, and re-layouts  4.4 us

profile of v2, /device:TPU:10, one launch (start us, length us, event | category | flops | bytes accessed | tf_op | source)
XLA Modules:
  0.0 124.4 jit_solution(13979715403656771120)
XLA Ops:
  0.0 1.3 %broadcast_in_dim.10.gain = bf16[1,2048]{1,0:T(2,128)(2,1)} reshape(bf16[2048]{0:T(1024)(128)(2,1)} %param.20) | data formatting | bytes 8192 | tf_op jit(solution)/shard_map/broadcast_in_dim | solution.py:451
  1.3 1.4 %copy.14.ids = s32[64,2]{1,0:T(8,128)} copy(s32[64,2]{0,1:T(2,128)} %param.21) | data formatting | bytes 1024 | tf_op args[8]
  2.6 1.4 %copy.15.route = f32[64,2]{1,0:T(8,128)} copy(f32[64,2]{0,1:T(2,128)} %param.22) | data formatting | bytes 1024 | tf_op args[9]
  4.0 1.5 %broadcast_in_dim.4.docs = s32[512,128]{1,0:T(8,128)} broadcast(s32[512]{0:T(512)} %param.17), dimensions={0} | broadcast | bytes 264192 | tf_op jit(solution)/shard_map/broadcast_in_dim | solution.py:449
  5.5 117.1 %shard_map.127 = bf16[64,2048]{1,0:T(8,128)(2,1)} custom-call(bf16[512,128]{1,0:T(8,128)(2,1)} %gb.1, bf16[512,128]{1,0:T(8,128)(2,1)} %gc.1, bf16[512,128]{1,0:T(8,128)(2,1)} %vals.1, bf16[3,128]{1,0:T(4,128)(2,1)} %taps.1, s32[512,128]{1,0:T(8,128)} %broadcast_in_dim.4.docs, bf16[64,2048]{1,0:T(8,128)(2,1)} %resid.1, ...), custom_call_target="tpu_custom_call" | custom-call | tf_op jit(solution)/shard_map/pallas_call | solution.py:381
  122.7 1.7 %copy.17 = bf16[64,2048]{1,0:T(8,128)(2,1)} copy(bf16[64,2048]{1,0:T(8,128)(2,1)} %shard_map.127) | data formatting | bytes 524288
